TPU v7x, 256 devices: a 4x2x16 block of a 4x16x16 slice. The times are simulated.
256 devices in a mesh: grp: 2 (over y), ep: 32 (over z, core), tp: 4 (over x).
Axes of the slice: x: 4, y: 2, z: 16, core: 2. Of those that a mesh axis runs over, the one named last changes fastest.
The devices are a block of a 4x16x16 slice.
Arguments:
- queries: bfloat16 [24576, 1024], P(('grp', 'ep'), 'tp'), parts along dimension 0, may hold values from -6 to 6
- key_values: bfloat16 [24576, 512], P(('grp', 'ep'), 'tp'), parts along dimension 0, may hold values from -6 to 6
- query_gain: float32 [64], replicated, may hold values from 0.5 to 5
- key_gain: float32 [64], replicated, may hold values from 0.5 to 5
- out_weight: bfloat16 [1024, 2048], P('tp'), may hold values from -0.1875 to 0.1875
- second_batch: bfloat16 [32768, 2048], P(('grp', 'ep', 'tp')), parts along dimension 0, may hold values from -6 to 6
- norm_gain: float32 [2048], replicated, may hold values from 0.1 to 1.9
- routes: int32 [32768, 2], P(('grp', 'ep', 'tp')), parts along dimension 0, may hold values from 0 to 63, all different within a row; in each aligned block of 128 rows (0 to 127, 128 to 255, ...) at most 6 rows name the same one
- route_weights: float32 [32768, 2], P(('grp', 'ep', 'tp')), parts along dimension 0, may hold values from 0.2 to 1
- expert_gate: bfloat16 [64, 2048, 1024], P('ep', None, 'tp'), may hold values from -0.125 to 0.125
- expert_up: bfloat16 [64, 2048, 1024], P('ep', None, 'tp'), may hold values from -0.125 to 0.125
- expert_down: bfloat16 [64, 1024, 2048], P('ep', 'tp'), may hold values from -0.1875 to 0.1875
- shared_gate: bfloat16 [2048, 512], P(None, 'tp'), may hold values from -0.125 to 0.125
- shared_up: bfloat16 [2048, 512], P(None, 'tp'), may hold values from -0.125 to 0.125
- shared_down: bfloat16 [512, 2048], P('tp'), may hold values from -0.25 to 0.25
Outputs:
- mixer_out: bfloat16 [24576, 2048], P(('grp', 'ep', 'tp')), parts along dimension 0
- channel_out: bfloat16 [32768, 2048], P(('grp', 'ep', 'tp')), parts along dimension 0
There are 2 independent parts, one for each index of `grp`. A program takes and returns all parts, laid end to end along the dimension named above; an argument that names none is the same for every part. Nothing has to cross between parts.
Inputs may be any that keep to these rules, and one draw needn't show every extreme that they name: `routes`: each row names 2 different experts. Among the rows of one device no expert is named more than 6 times, and in every draw some expert is named exactly 6 times by the rows of some device.
All inputs are finite; a program needn't handle non-finite values.
Results may differ from a plain program's by a relative error of at most 0.015.
The roundings to bfloat16 on the way count: a program that leaves them out, or rounds other values in their place, can miss the bound.
Values may be sent and summed in bfloat16 or wider, within the bound.
A program may use at most 128 MiB of HBM per device.

v0:
```python
import jax
import jax.numpy as jnp
from jax import lax
from jax.sharding import Mesh
from jax.sharding import PartitionSpec as P

GRID_W = 64
EP = ("ep_0", "ep_1")
GRP_EP = ("grp", "ep_0", "ep_1")
GRP_EP_TP = ("grp", "ep_0", "ep_1", "tp")
rope_base = 10000.0
norm_eps = 1e-06


def joined_along(tiles, dim):
    shape = list(tiles.shape[1:])
    shape[dim] *= tiles.shape[0]
    return jnp.moveaxis(tiles, 0, dim).reshape(shape)


def stacked_from(shard, axes, order):
    tiles = shard
    for k in order:
        tiles = lax.all_gather(tiles, axes[k])
    done = order[::-1]
    back = [done.index(k) for k in range(len(axes))]
    tiles = tiles.transpose(*back, *range(len(axes), tiles.ndim))
    return tiles.reshape(-1, *shard.shape)


def whole_of(shard, axes, order, dim):
    return joined_along(stacked_from(shard, axes, order), dim)


def from_everyone(shard, axis):
    copies = jnp.broadcast_to(shard, (lax.axis_size(axis), *shard.shape))
    return lax.all_to_all(copies, axis, split_axis=0, concat_axis=0, tiled=True)


def gathered_copies(shard, axis, dim):
    return joined_along(from_everyone(shard, axis), dim)


def in_blocks(shard, dim, length):
    shape = shard.shape
    tiles = shard.reshape(*shape[:dim], length, shape[dim] // length, *shape[dim + 1 :])
    return jnp.moveaxis(tiles, dim, 0)


def summed_on_arrival(shard, axis, dim):
    tiles = in_blocks(shard, dim, lax.axis_size(axis))
    arrived = lax.all_to_all(tiles, axis, split_axis=0, concat_axis=0, tiled=True)
    return arrived.astype(jnp.float32).sum(axis=0)


def head_norm(vectors, gain):
    return (
        vectors * lax.rsqrt(jnp.mean(vectors * vectors, axis=-1, keepdims=True) + norm_eps) * gain
    )


def turn_heads(vectors, positions):
    row_count, head_count, head_size = vectors.shape
    half_size = head_size // 2
    inverse = rope_base ** (-jnp.arange(0, half_size, 2, dtype=jnp.float32) / half_size)
    grid_row = (positions // GRID_W).astype(jnp.float32)
    grid_column = (positions % GRID_W).astype(jnp.float32)
    angles = jnp.concatenate([grid_row[:, None] * inverse, grid_column[:, None] * inverse], axis=-1)
    cosine = jnp.cos(angles)[:, None, :]
    sine = jnp.sin(angles)[:, None, :]
    paired = vectors.reshape(row_count, head_count, half_size, 2)
    first = paired[..., 0]
    second = paired[..., 1]
    turned = jnp.stack([first * cosine - second * sine, first * sine + second * cosine], axis=-1)
    return turned.reshape(vectors.shape)


def slot_ids(route_rows, expert_count, capacity):
    row_count, top_count = route_rows.shape
    flat_routes = route_rows.reshape(-1)
    onehot = (flat_routes[:, None] == jnp.arange(expert_count, dtype=jnp.int32)[None, :]).astype(
        jnp.int32
    )
    earlier = jnp.cumsum(onehot, axis=0) - onehot
    within = jnp.sum(earlier * onehot, axis=1)
    return (flat_routes * capacity + within).reshape(row_count, top_count)


def slot_table(slots, slot_count):
    row_count, top_count = slots.shape
    flat_slots = slots.reshape(-1)
    owner_row = jnp.arange(row_count * top_count, dtype=jnp.int32) // top_count
    matches = flat_slots[None, :] == jnp.arange(slot_count, dtype=jnp.int32)[:, None]
    occupied = jnp.any(matches, axis=1)
    source_row = jnp.sum(jnp.where(matches, owner_row[None, :], 0), axis=1)
    return jnp.where(occupied, source_row, row_count)


def pick_block(row_count):
    for candidate in range(min(row_count, 1024), 0, -1):
        if row_count % candidate == 0:
            return candidate
    return row_count


def attend_keys(query_turned, scale, running, pieces):
    head_size = query_turned.shape[-1]
    key_block = pick_block(pieces.shape[0])
    blocks = pieces.reshape(pieces.shape[0] // key_block, key_block, 2 * head_size)

    def one_block(carried, block_rows):
        top_now, total_now, acc_now = carried
        scores = (
            jnp.einsum(
                "qhd,kd->hqk",
                query_turned,
                block_rows[:, :head_size],
                preferred_element_type=jnp.float32,
            )
            * scale
        )
        top_new = jnp.maximum(top_now, jnp.max(scores, axis=-1))
        shrink = jnp.exp(top_now - top_new)
        exps = jnp.exp(scores - top_new[..., None])
        total_new = total_now * shrink + jnp.sum(exps, axis=-1)
        acc_new = acc_now * shrink[..., None] + jnp.einsum(
            "hqk,kd->hqd",
            exps.astype(jnp.bfloat16),
            block_rows[:, head_size:],
            preferred_element_type=jnp.float32,
        )
        return ((top_new, total_new, acc_new), None)

    result, ignored = lax.scan(one_block, running, blocks)
    return result


def shared_hidden_of(token_rows, gate_weights, up_weights):
    gate_part = jnp.dot(token_rows, gate_weights, preferred_element_type=jnp.float32)
    up_part = jnp.dot(token_rows, up_weights, preferred_element_type=jnp.float32)
    return (jax.nn.silu(gate_part) * up_part).astype(jnp.bfloat16)


def expert_hidden(slot_rows, gate_weights, up_weights):
    gate_part = jnp.einsum(
        "osjcd,jdf->osjcf", slot_rows, gate_weights, preferred_element_type=jnp.float32
    )
    up_part = jnp.einsum(
        "osjcd,jdf->osjcf", slot_rows, up_weights, preferred_element_type=jnp.float32
    )
    return (jax.nn.silu(gate_part) * up_part).astype(jnp.bfloat16)


def body(
    queries,
    key_values,
    query_gain,
    key_gain,
    out_weight,
    second_batch,
    norm_gain,
    routes,
    route_weights,
    expert_gate,
    expert_up,
    expert_down,
    shared_gate,
    shared_up,
    shared_down,
):
    query_rows = queries.shape[0]
    head_size = query_gain.shape[0]
    heads_here = queries.shape[1] // head_size
    ep_count = lax.axis_size(EP)
    positions = lax.axis_index(EP) * query_rows + jnp.arange(query_rows, dtype=jnp.int32)
    query_turned = turn_heads(
        head_norm(
            queries.reshape(query_rows, heads_here, head_size).astype(jnp.float32), query_gain
        ),
        positions,
    ).astype(jnp.bfloat16)
    key_turned = turn_heads(
        head_norm(key_values[:, None, :head_size].astype(jnp.float32), key_gain), positions
    ).astype(jnp.bfloat16)
    keys_and_values = jnp.concatenate([key_turned[:, 0, :], key_values[:, head_size:]], axis=1)
    start_state = (
        jnp.full((heads_here, query_rows), -1e30, jnp.float32),
        jnp.zeros((heads_here, query_rows), jnp.float32),
        jnp.zeros((heads_here, query_rows, head_size), jnp.float32),
    )
    top_all, total_all, acc_all = attend_keys(
        query_turned, head_size ** (-0.5), start_state, whole_of(keys_and_values, EP, (0, 1), 0)
    )
    head_out = (
        (acc_all / total_all[..., None])
        .transpose(1, 0, 2)
        .reshape(query_rows, heads_here * head_size)
        .astype(jnp.bfloat16)
    )
    tok_count = second_batch.shape[0]
    model_width = second_batch.shape[1]
    top_count = routes.shape[1]
    local_experts = expert_gate.shape[0]
    expert_count = local_experts * ep_count
    capacity = 3 * tok_count * top_count // (2 * expert_count)
    slot_count = expert_count * capacity
    token_float = second_batch.astype(jnp.float32)
    normed = (
        token_float
        * lax.rsqrt(jnp.mean(token_float * token_float, axis=-1, keepdims=True) + norm_eps)
        * norm_gain
    ).astype(jnp.bfloat16)
    own_slots = slot_ids(routes, expert_count, capacity)
    shared_hidden = (lambda pieces, begin_at: shared_hidden_of(pieces, shared_gate, shared_up))(
        gathered_copies(normed, "tp", 0), jnp.int32(0)
    )
    outgoing = jnp.take(
        normed, slot_table(own_slots, slot_count), axis=0, mode="fill", fill_value=0
    )[None]
    arrived = lax.all_to_all(outgoing, EP, split_axis=1, concat_axis=1, tiled=True)
    arrived = arrived.reshape(arrived.shape[0], ep_count, local_experts, capacity, model_width)
    hidden = expert_hidden(
        lax.all_gather(arrived, "tp", axis=0, tiled=True), expert_gate, expert_up
    )
    routed_part = jnp.einsum(
        "osjcf,jfd->osjcd", hidden, expert_down, preferred_element_type=jnp.float32
    ).reshape(-1, model_width)
    shared_part = jnp.dot(shared_hidden, shared_down, preferred_element_type=jnp.float32)
    head_partial = jnp.dot(head_out, out_weight, preferred_element_type=jnp.float32)
    attn_sum, routed_sum, shared_sum = (
        summed_on_arrival(head_partial.astype(jnp.bfloat16), "tp", 0),
        summed_on_arrival(routed_part.astype(jnp.bfloat16), "tp", 0),
        summed_on_arrival(shared_part.astype(jnp.bfloat16), "tp", 0),
    )
    returned = lax.all_to_all(
        routed_sum.astype(jnp.bfloat16), EP, split_axis=0, concat_axis=0, tiled=True
    )
    combined = shared_sum
    for slot_pick in range(top_count):
        combined = combined + route_weights[:, slot_pick : slot_pick + 1] * jnp.take(
            returned, own_slots[:, slot_pick], axis=0
        ).astype(jnp.float32)
    return (attn_sum.astype(jnp.bfloat16), combined.astype(jnp.bfloat16))


def solution(mesh):
    torus = Mesh(
        mesh.devices.reshape(mesh.shape["grp"], 16, 2, mesh.shape["tp"]),
        ("grp", "ep_0", "ep_1", "tp"),
    )
    return jax.shard_map(
        body,
        mesh=torus,
        in_specs=(
            P(GRP_EP, "tp"),
            P(GRP_EP, "tp"),
            P(),
            P(),
            P("tp", None),
            P(GRP_EP_TP, None),
            P(),
            P(GRP_EP_TP, None),
            P(GRP_EP_TP, None),
            P(EP, None, "tp"),
            P(EP, None, "tp"),
            P(EP, "tp", None),
            P(None, "tp"),
            P(None, "tp"),
            P("tp", None),
        ),
        out_specs=(P(GRP_EP_TP, None), P(GRP_EP_TP, None)),
        check_vma=False,
    )
```

profile of v0, /device:TPU:33, one launch (start us, length us, event | category | flops | bytes accessed | tf_op | source)
XLA Modules:
  0.0 621.9 jit_solution(13244901644372939689)
XLA Ops:
  12.2 3.3 gather_fusion
  15.5 1.6 bitcast_select_fusion
  17.1 4.1 copy.120
  21.7 12.4 %reduce.10 = bf16[384,2048]{1,0:T(8,128)(2,1)} reduce(bf16[384,1,2048]{2,1,0:T(2,128)(2,1)} %bitcast.152, bf16[]{:T(256)} %broadcast.416), dimensions={1}, to_apply=%bitcast.134.reduce_sub_computation | reduce | bytes 3145730
  34.1 5.2 reshape.492
  39.3 25.6 %all-to-all-start.3 = ((bf16[32,2,12288]{2,1,0:T(2,128)(2,1)}), bf16[32,2,12288]{2,1,0:T(2,128)(2,1)}, u32[]{:S(2)}, u32[]{:S(2)}) async-start(bf16[32,2,12288]{2,1,0:T(2,128)(2,1)} %reshape.492), calls=%async_computation.3 | async-start | bytes 3145728 | tf_op jit(solution)/shard_map/all_to_all | solution.py:220
  66.8 95.3 %all-gather.8.cloned.1.call-done = bf16[6144,128]{0,1:T(8,128)(2,1)} async-done(((bf16[384,128]{0,1:T(8,128)(2,1)}), bf16[6144,128]{0,1:T(8,128)(2,1)}) %all-gather.8.cloned.1.call-update) | async-done | bytes 1572880 | tf_op jit(solution)/shard_map/all_gather | solution.py:24
  162.1 2.6 copy.106
  164.9 9.5 %reshape.493 = bf16[384,1,2048]{2,1,0:T(2,128)(2,1)} reshape(bf16[32,2,12288]{2,1,0:T(2,128)(2,1)} %all-to-all-done.3) | data formatting | bytes 3145728
  174.3 12.2 %bitcast_reduce_fusion.2 = bf16[384,2048]{1,0:T(8,128)(2,1)} fusion(bf16[384,1,2048]{2,1,0:T(2,128)(2,1)} %reshape.493), kind=kLoop, calls=%fused_computation.129 | loop fusion | bytes 3145728 | tf_op jit(solution)/shard_map/all_to_all | solution.py:220
  186.6 3.7 reshape.450
  190.3 3.6 copy.99
  194.0 1.7 broadcast_in_dim.47
  195.7 4.8 all-to-all-start.1
  202.6 25.4 %all-to-all-done.1 = bf16[4,128,2048]{2,1,0:T(8,128)(2,1)} async-done(((bf16[4,128,2048]{2,1,0:T(8,128)(2,1)}), bf16[4,128,2048]{2,1,0:T(8,128)(2,1)}, u32[]{:S(2)}, u32[]{:S(2)}) %all-to-all-start.1) | async-done | bytes 2097184 | tf_op jit(solution)/shard_map/all_to_all | solution.py:37
  227.9 2.4 fusion.58
  230.3 5.5 convolution_convert_fusion
  235.8 4.5 all-to-all-start.2
  240.4 4.0 copy.91
  244.4 55.9 %all-gather.6.cloned.1.call-done = bf16[4,32,2,6,2048]{4,1,3,0,2:T(8,128)(2,1)} async-done(((bf16[1,32,2,6,2048]{4,1,3,0,2:T(8,128)(2,1)}), bf16[4,32,2,6,2048]{4,1,3,0,2:T(8,128)(2,1)}) %all-gather.6.cloned.1.call-update) | async-done | bytes 6291472 | tf_op jit(solution)/shard_map/all_gather | solution.py:223
  300.3 6.4 %fusion.14 = f32[2,4,32,6,256]{4,2,3,1,0:T(8,128)} fusion(bf16[4,32,2,6,2048]{4,1,3,0,2:T(8,128)(2,1)} %all-gather.6.cloned.1.call-done, bf16[2,2048,256]{2,1,0:T(8,128)(2,1)} %param.28), kind=kOutput, calls=%fused_computation.27 | convolution fusion | flops 1610612736 | bytes 9961472 | tf_op jit(solution)/shard_map/osjcd,jdf->osjcf/dot_general | solution.py:145
  306.7 10.1 %convert_bitcast_fusion = bf16[4,32,2,6,2048]{4,1,3,0,2:T(8,128)(2,1)} fusion(bf16[2,256,2048]{2,1,0:T(8,128)(2,1)S(1)} %copy-done, f32[2,4,32,6,256]{4,2,3,1,0:T(8,128)} %fusion.14, bf16[4,32,2,6,2048]{4,1,3,0,2:T(8,128)(2,1)} %all-gather.6.cloned.1.call-done, bf16[2,2048,256]{2,1,0:T(8,128)(2,1)} %param.29), kind=kOutput, calls=%fused_computation.20 | convolution fusion | flops 3226730496 | bytes 18350080 | tf_op jit(solution)/shard_map/osjcf,jfd->osjcd/dot_general | solution.py:225
  316.8 10.2 %copy.100 = bf16[4,32,2,6,2048]{4,0,3,2,1:T(4,128)(2,1)} copy(bf16[4,32,2,6,2048]{4,1,3,0,2:T(8,128)(2,1)} %convert_bitcast_fusion) | data formatting | bytes 12582912 | tf_op jit(solution)/shard_map/convert_element_type | solution.py:232
  327.0 9.1 %copy.101 = bf16[4,384,2048]{2,1,0:T(8,128)(2,1)} copy(bf16[4,384,2048]{2,0,1:T(4,128)(2,1)} %bitcast.151) | data formatting | bytes 12582912 | tf_op jit(solution)/shard_map/convert_element_type | solution.py:232
  336.1 5.3 all-to-all-start.4
  341.5 127.8 %while.15 = (s32[]{:T(128)}, f32[4,384]{1,0:T(4,128)S(1)}, f32[4,384]{1,0:T(4,128)S(1)}, f32[4,384,64]{1,2,0:T(8,128)S(1)}, bf16[12,1024,128]{2,1,0:T(8,128)(2,1...) while((s32[]{:T(128)}, f32[4,384]{1,0:T(4,128)S(1)}, f32[4,384]{1,0:T(4,128)S(1)}, ...), condition=%wide.region_5.6_spmd.clone, body=%wide.region_2.5_spmd.clone.sunk | while | flops 415538688 | bytes 46432384 | solution.py:134
  342.7 3.6 bitcast_reduce_fusion.4
  346.3 4.0 fusion.76
  353.3 3.6 bitcast_reduce_fusion.4
  357.0 4.0 fusion.76
  364.0 3.6 bitcast_reduce_fusion.4
  367.6 4.0 fusion.76
  372.2 1.3 fusion.78
  374.6 3.6 bitcast_reduce_fusion.4
  378.2 4.0 fusion.76
  382.8 1.3 fusion.78
  385.3 3.6 bitcast_reduce_fusion.4
  388.9 4.0 fusion.76
  395.9 3.6 bitcast_reduce_fusion.4
  399.5 4.0 fusion.76
  406.5 3.6 bitcast_reduce_fusion.4
  410.2 4.0 fusion.76
  417.2 3.6 bitcast_reduce_fusion.4
  420.8 4.0 fusion.76
  427.8 3.6 bitcast_reduce_fusion.4
  431.5 4.0 fusion.76
  438.5 3.6 bitcast_reduce_fusion.4
  442.1 4.0 fusion.76
  449.1 3.6 bitcast_reduce_fusion.4
  452.8 4.0 fusion.76
  459.8 3.6 bitcast_reduce_fusion.4
  463.4 4.0 fusion.76
  469.3 1.8 convolution_convert_fusion.1
  471.1 4.1 all-to-all-start
  475.3 5.7 reduce_sum.96
  480.9 3.6 all_to_all.28
  484.5 10.4 %all-to-all-done = bf16[4,96,2048]{2,1,0:T(8,128)(2,1)S(1)} async-done(((bf16[4,96,2048]{2,1,0:T(8,128)(2,1)}), bf16[4,96,2048]{2,1,0:T(8,128)(2,1)S(1)}, u32[]{:S(2)}, u32[]{:S(2)}) %all-to-all-start) | async-done | bytes 1572896 | tf_op jit(solution)/shard_map/all_to_all | solution.py:52
  495.0 11.2 %all-to-all-start.5 = ((bf16[32,12,2048]{2,1,0:T(8,128)(2,1)}), bf16[32,12,2048]{2,1,0:T(8,128)(2,1)}, u32[]{:S(2)}, u32[]{:S(2)}) async-start(bf16[32,12,2048]{2,1,0:T(8,128)(2,1)} %all_to_all.28), calls=%async_computation.5 | async-start | bytes 4194304 | tf_op jit(solution)/shard_map/all_to_all | solution.py:235
  506.4 2.1 convert_reduce_fusion
  509.6 94.8 %all-to-all-done.5 = bf16[32,12,2048]{2,1,0:T(8,128)(2,1)} async-done(((bf16[32,12,2048]{2,1,0:T(8,128)(2,1)}), bf16[32,12,2048]{2,1,0:T(8,128)(2,1)}, u32[]{:S(2)}, u32[]{:S(2)}) %all-to-all-start.5) | async-done | bytes 1572896 | tf_op jit(solution)/shard_map/all_to_all | solution.py:235
  604.4 2.5 all_to_all.30
  606.9 1.7 gather_fusion.1
  608.7 4.0 gather_fusion.2
  612.7 2.4 add_convert_fusion
  (180 shorter events, 44.5 us)
Async XLA Ops:
  7.2 299.5 %copy-start = (bf16[2,256,2048]{2,1,0:T(8,128)(2,1)S(1)}, bf16[2,256,2048]{2,1,0:T(8,128)(2,1)}, u32[]{:S(2)}) copy-start(bf16[2,256,2048]{2,1,0:T(8,128)(2,1)} %param.30) | copy-start | bytes 6291460
  39.3 25.7 %copy-start.5 = (bf16[384,128]{1,0:T(8,128)(2,1)S(1)}, bf16[384,128]{1,0:T(8,128)(2,1)}, u32[]{:S(2)}) copy-start(bf16[384,128]{1,0:T(8,128)(2,1)} %param.20) | copy-start | bytes 294916
  39.3 26.0 %copy-start.9 = (f32[64]{0:T(128)S(1)}, f32[64]{0:T(128)}, u32[]{:S(2)}) copy-start(f32[64]{0:T(128)} %param.22) | copy-start | bytes 772
  39.3 125.6 %all-to-all-start.3 = ((bf16[32,2,12288]{2,1,0:T(2,128)(2,1)}), bf16[32,2,12288]{2,1,0:T(2,128)(2,1)}, u32[]{:S(2)}, u32[]{:S(2)}) async-start(bf16[32,2,12288]{2,1,0:T(2,128)(2,1)} %reshape.492), calls=%async_computation.3 | async-start | bytes 3145728 | tf_op jit(solution)/shard_map/all_to_all | solution.py:220
  64.9 97.2 %all-gather.8.cloned.1.call-start = ((), (), s32[]{:S(2)}) async-start(), calls=%async_computation.7 | async-start | bytes 1671168 | tf_op jit(solution)/shard_map/all_gather | solution.py:24
  66.7 173.7 %all-gather.10.cloned.1.call-start = ((), (), s32[]{:S(2)}) async-start(), calls=%async_computation.8 | async-start | bytes 4718592 | tf_op jit(solution)/shard_map/all_gather | solution.py:24
  164.8 135.5 %all-gather.6.cloned.1.call-start = ((), (), s32[]{:S(2)}) async-start(), calls=%async_computation.6 | async-start | bytes 7864320 | tf_op jit(solution)/shard_map/all_gather | solution.py:223
  195.7 4.9 copy-start.6
  195.7 5.3 copy-start.10
  195.7 32.2 %all-to-all-start.1 = ((bf16[4,128,2048]{2,1,0:T(8,128)(2,1)}), bf16[4,128,2048]{2,1,0:T(8,128)(2,1)}, u32[]{:S(2)}, u32[]{:S(2)}) async-start(bf16[4,128,2048]{2,1,0:T(8,128)(2,1)} %broadcast_in_dim.47), calls=%async_computation.1 | async-start | bytes 4194304 | tf_op jit(solution)/shard_map/all_to_all | solution.py:37
  235.8 100.3 %all-to-all-start.2 = ((bf16[4,128,2048]{2,1,0:T(8,128)(2,1)}), bf16[4,128,2048]{2,1,0:T(8,128)(2,1)}, u32[]{:S(2)}, u32[]{:S(2)}) async-start(bf16[4,128,2048]{2,1,0:T(8,128)(2,1)} %bitcast.153), calls=%async_computation.2 | async-start | bytes 4194304 | tf_op jit(solution)/shard_map/all_to_all | solution.py:52
  336.1 135.0 %all-to-all-start.4 = ((bf16[4,384,2048]{2,1,0:T(8,128)(2,1)}), bf16[4,384,2048]{2,1,0:T(8,128)(2,1)}, u32[]{:S(2)}, u32[]{:S(2)}) async-start(bf16[4,384,2048]{2,1,0:T(8,128)(2,1)} %copy.101), calls=%async_computation.4 | async-start | bytes 12582912 | tf_op jit(solution)/shard_map/all_to_all | solution.py:52
  341.4 127.9 %copy-start.4 = (bf16[256,2048]{1,0:T(8,128)(2,1)S(1)}, bf16[256,2048]{1,0:T(8,128)(2,1)}, u32[]{:S(2)}) copy-start(bf16[256,2048]{1,0:T(8,128)(2,1)} %param.23) | copy-start | bytes 3145732
  346.3 4.6 copy-start.2
  357.0 4.6 copy-start.2
  367.6 4.6 copy-start.2
  378.2 4.6 copy-start.2
  388.9 4.6 copy-start.2
  399.5 4.6 copy-start.2
  410.2 4.6 copy-start.2
  420.8 4.6 copy-start.2
  431.5 4.6 copy-start.2
  442.1 4.6 copy-start.2
  452.7 4.6 copy-start.2
  463.4 4.6 copy-start.2
  471.1 23.9 %all-to-all-start = ((bf16[4,96,2048]{2,1,0:T(8,128)(2,1)}), bf16[4,96,2048]{2,1,0:T(8,128)(2,1)S(1)}, u32[]{:S(2)}, u32[]{:S(2)}) async-start(bf16[4,96,2048]{2,1,0:T(8,128)(2,1)} %bitcast.156), calls=%async_computation | async-start | bytes 3145728 | tf_op jit(solution)/shard_map/all_to_all | solution.py:52
  484.5 21.8 %copy-start.7 = (s32[128,2]{0,1:T(2,128)S(1)}, s32[128,2]{0,1:T(2,128)}, u32[]{:S(2)}) copy-start(s32[128,2]{0,1:T(2,128)} %param.26) | copy-start | bytes 3076
  484.5 21.9 %copy-start.8 = (f32[128,2]{0,1:T(2,128)S(1)}, f32[128,2]{0,1:T(2,128)}, u32[]{:S(2)}) copy-start(f32[128,2]{0,1:T(2,128)} %param.27) | copy-start | bytes 3076
  495.0 109.4 %all-to-all-start.5 = ((bf16[32,12,2048]{2,1,0:T(8,128)(2,1)}), bf16[32,12,2048]{2,1,0:T(8,128)(2,1)}, u32[]{:S(2)}, u32[]{:S(2)}) async-start(bf16[32,12,2048]{2,1,0:T(8,128)(2,1)} %all_to_all.28), calls=%async_computation.5 | async-start | bytes 4194304 | tf_op jit(solution)/shard_map/all_to_all | solution.py:235
  606.9 1.8 copy-start.3
  608.7 6.4 %copy-start.1 = (bf16[2,256,2048]{2,1,0:T(8,128)(2,1)S(1)}, bf16[2,256,2048]{2,1,0:T(8,128)(2,1)}, u32[]{:S(2)}) copy-start(bf16[2,256,2048]{2,1,0:T(8,128)(2,1)} %param.30) | copy-start | bytes 6291460
Sparse Core Ops, SparseCore 0:
  68.1 93.9 all-gather.7
  164.9 24.2 all-gather.9
  194.1 106.1 all-gather.5
where the time goes:
time: 626 us; the launch traced here: 622 us
  waiting for transfers between devices  282 us (45%)
  local copies, waits for them, and re-layouts  105 us (17%)
  matrix products  84.7 us (14%)
  other arithmetic  79.3 us (13%)
  starting transfers between devices  55.8 us (9%)
  between operations  14.5 us (2%)
    all_gather x2, waiting for transfers between devices, stacked_from(): tiles = lax.all_gather(tiles, axes[k])  95.4 us
    all_to_all x1, waiting for transfers between devices, body(): lax.all_to_all(routed_sum.astype(jnp.bfloat16), EP, split_axis=0, concat_...  94.8 us
    all_gather x1, waiting for transfers between devices, body(): lax.all_gather(arrived, 'tp', axis=0, tiled=True)  55.9 us
    reduce_sum x12, other arithmetic, one_block(): total_new = total_now * shrink + jnp.sum(exps, axis=-1)  47.6 us
    dot_general x12, matrix products, one_block(): jnp.einsum('qhd,kd->hqk', query_turned, block_rows[:, :head_size], prefer...  43.5 us
    all_to_all x1, starting transfers between devices, body(): lax.all_to_all(outgoing, EP, split_axis=1, concat_axis=1, tiled=True)  25.6 us
    all_to_all x1, waiting for transfers between devices, from_everyone(): return lax.all_to_all(copies, axis, split_axis=0, concat_axis=0, tiled=True)  25.4 us
    convert_element_type x2, local copies, waits for them, and re-layouts, body(): routed_part.astype(jnp.bfloat16)  19.3 us
  transfers between devices with their start and end apart: 9, of which 5 were waited for; matrix products, arithmetic and copies ran while one was open for 35% of the time, Pallas kernels for 0%

commit v1 on v0

--- a/solution.py
+++ b/solution.py
@@ -217,7 +217,9 @@
     outgoing = jnp.take(
         normed, slot_table(own_slots, slot_count), axis=0, mode="fill", fill_value=0
     )[None]
-    arrived = lax.all_to_all(outgoing, EP, split_axis=1, concat_axis=1, tiled=True)
+    arrived = jnp.concatenate(
+        lax.all_to_all(jnp.stack(jnp.split(outgoing, lax.axis_size(EP), axis=1)), EP, 0, 0), axis=1
+    )
     arrived = arrived.reshape(arrived.shape[0], ep_count, local_experts, capacity, model_width)
     hidden = expert_hidden(
         lax.all_gather(arrived, "tp", axis=0, tiled=True), expert_gate, expert_up

time: 626 us -> 598 us (0.955)
  local copies, waits for them, and re-layouts: 105 us -> 90.2 us
  other arithmetic: 79.3 us -> 65.5 us
    all_to_all x1, waiting for transfers between devices: 0.01 us -> 55.8 us  [body(): lax.all_to_all(jnp.stack(jnp.split(outgoing, lax.axis_size(EP), axis=1)),...]
    all_gather x2, waiting for transfers between devices: 95.4 us -> 45.3 us  [stacked_from(): tiles = lax.all_gather(tiles, axes[k])]
    unnamed x4 -> x3, other arithmetic: 12.4 us -> 0.01 us
    all_to_all x1, waiting for transfers between devices: 25.4 us -> 37.5 us  [from_everyone(): return lax.all_to_all(copies, axis, split_axis=0, concat_axis=0, tiled=True)]
    all_gather x1, waiting for transfers between devices: 55.9 us -> 43.9 us  [body(): lax.all_gather(arrived, 'tp', axis=0, tiled=True)]
    all_to_all x1, local copies, waits for them, and re-layouts: 12.2 us -> 3.62 us  [body(): lax.all_to_all(jnp.stack(jnp.split(outgoing, lax.axis_size(EP), axis=1)),...]
    reshape x2 -> x0, local copies, waits for them, and re-layouts: 7.34 us -> none  [body(): arrived.reshape(arrived.shape[0], ep_count, local_experts, capacity, mode...]
    unnamed x27 -> x55, local copies, waits for them, and re-layouts: 16.6 us -> 20.3 us
  transfers between devices with their start and end apart: 9 -> 9, of which waited for: 5 -> 6; matrix products, arithmetic and copies ran while one was open for 35% -> 36% of each run, Pallas kernels for 0% -> 0%
where the time goes in v1:
time: 598 us; the launch traced here: 596 us
  waiting for transfers between devices  288 us (48%)
  local copies, waits for them, and re-layouts  90.2 us (15%)
  matrix products  84.5 us (14%)
  other arithmetic  65.5 us (11%)
  starting transfers between devices  53 us (9%)
  between operations  14.2 us (2%)
    all_to_all x1, waiting for transfers between devices, body(): lax.all_to_all(routed_sum.astype(jnp.bfloat16), EP, split_axis=0, concat_...  95.3 us
    all_to_all x1, waiting for transfers between devices, body(): lax.all_to_all(jnp.stack(jnp.split(outgoing, lax.axis_size(EP), axis=1)),...  55.8 us
    reduce_sum x12, other arithmetic, one_block(): total_new = total_now * shrink + jnp.sum(exps, axis=-1)  47.6 us
    all_gather x2, waiting for transfers between devices, stacked_from(): tiles = lax.all_gather(tiles, axes[k])  45.3 us
    all_gather x1, waiting for transfers between devices, body(): lax.all_gather(arrived, 'tp', axis=0, tiled=True)  43.9 us
    dot_general x12, matrix products, one_block(): jnp.einsum('qhd,kd->hqk', query_turned, block_rows[:, :head_size], prefer...  43.2 us
    all_to_all x1, waiting for transfers between devices, from_everyone(): return lax.all_to_all(copies, axis, split_axis=0, concat_axis=0, tiled=True)  37.5 us
    all_to_all x1, starting transfers between devices, body(): lax.all_to_all(jnp.stack(jnp.split(outgoing, lax.axis_size(EP), axis=1)),...  25.5 us
  transfers between devices with their start and end apart: 9, of which 6 were waited for; matrix products, arithmetic and copies ran while one was open for 36% of the time, Pallas kernels for 0%

profile of v1, /device:TPU:33, one launch (start us, length us, event | category | flops | bytes accessed | tf_op | source)
XLA Modules:
  0.0 596.4 jit_solution(535935145309427397)
XLA Ops:
  12.9 3.1 gather_fusion
  16.0 1.6 bitcast_select_fusion
  38.0 25.5 %all-to-all-start.3 = ((bf16[32,1,12,2048]{3,2,1,0:T(8,128)(2,1)}), bf16[32,1,12,2048]{3,2,1,0:T(8,128)(2,1)}, u32[]{:S(2)}, u32[]{:S(2)}) async-start(bf16[32,1,12,2048]{3,2,1,0:T(8,128)(2,1)} %fusion.41), calls=%async_computation.3 | async-start | bytes 4194304 | tf_op jit(solution)/shard_map/all_to_all | solution.py:221
  63.6 45.3 %all-gather.8.cloned.1.call-done = bf16[6144,128]{0,1:T(8,128)(2,1)} async-done(((bf16[384,128]{0,1:T(8,128)(2,1)}), bf16[6144,128]{0,1:T(8,128)(2,1)}) %all-gather.8.cloned.1.call-update) | async-done | bytes 1572880 | tf_op jit(solution)/shard_map/all_gather | solution.py:24
  108.9 2.6 copy.104
  111.6 55.8 %all-to-all-done.3 = bf16[32,1,12,2048]{3,2,1,0:T(8,128)(2,1)} async-done(((bf16[32,1,12,2048]{3,2,1,0:T(8,128)(2,1)}), bf16[32,1,12,2048]{3,2,1,0:T(8,128)(2,1)}, u32[]{:S(2)}, u32[]{:S(2)}) %all-to-all-start.3) | async-done | bytes 1572896 | tf_op jit(solution)/shard_map/all_to_all | solution.py:221
  167.4 3.6 copy.97
  171.1 1.7 broadcast_in_dim.47
  172.8 4.7 all-to-all-start.1
  179.5 37.5 %all-to-all-done.1 = bf16[4,128,2048]{2,1,0:T(8,128)(2,1)} async-done(((bf16[4,128,2048]{2,1,0:T(8,128)(2,1)}), bf16[4,128,2048]{2,1,0:T(8,128)(2,1)}, u32[]{:S(2)}, u32[]{:S(2)}) %all-to-all-start.1) | async-done | bytes 2097184 | tf_op jit(solution)/shard_map/all_to_all | solution.py:37
  217.0 2.4 fusion.90
  219.4 5.5 convolution_convert_fusion
  224.9 4.8 all-to-all-start.2
  229.7 4.0 copy.90
  233.6 43.9 %all-gather.6.cloned.1.call-done = bf16[4,32,2,6,2048]{4,1,3,0,2:T(8,128)(2,1)} async-done(((bf16[1,32,2,6,2048]{4,1,3,0,2:T(8,128)(2,1)}), bf16[4,32,2,6,2048]{4,1,3,0,2:T(8,128)(2,1)}) %all-gather.6.cloned.1.call-update) | async-done | bytes 6291472 | tf_op jit(solution)/shard_map/all_gather | solution.py:225
  277.6 6.4 %fusion.14 = f32[2,4,32,6,256]{4,2,3,1,0:T(8,128)} fusion(bf16[4,32,2,6,2048]{4,1,3,0,2:T(8,128)(2,1)} %all-gather.6.cloned.1.call-done, bf16[2,2048,256]{2,1,0:T(8,128)(2,1)} %param.28), kind=kOutput, calls=%fused_computation.27 | convolution fusion | flops 1610612736 | bytes 9961472 | tf_op jit(solution)/shard_map/osjcd,jdf->osjcf/dot_general | solution.py:145
  284.0 10.1 %convert_bitcast_fusion = bf16[4,32,2,6,2048]{4,1,3,0,2:T(8,128)(2,1)} fusion(bf16[2,256,2048]{2,1,0:T(8,128)(2,1)S(1)} %copy-done, f32[2,4,32,6,256]{4,2,3,1,0:T(8,128)} %fusion.14, bf16[4,32,2,6,2048]{4,1,3,0,2:T(8,128)(2,1)} %all-gather.6.cloned.1.call-done, bf16[2,2048,256]{2,1,0:T(8,128)(2,1)} %param.29), kind=kOutput, calls=%fused_computation.20 | convolution fusion | flops 3226730496 | bytes 18350080 | tf_op jit(solution)/shard_map/osjcf,jfd->osjcd/dot_general | solution.py:227
  294.1 10.2 %copy.98 = bf16[4,32,2,6,2048]{4,0,3,2,1:T(4,128)(2,1)} copy(bf16[4,32,2,6,2048]{4,1,3,0,2:T(8,128)(2,1)} %convert_bitcast_fusion) | data formatting | bytes 12582912 | tf_op jit(solution)/shard_map/convert_element_type | solution.py:234
  304.3 9.1 %copy.99 = bf16[4,384,2048]{2,1,0:T(8,128)(2,1)} copy(bf16[4,384,2048]{2,0,1:T(4,128)(2,1)} %bitcast.275) | data formatting | bytes 12582912 | tf_op jit(solution)/shard_map/convert_element_type | solution.py:234
  313.4 5.3 all-to-all-start.4
  318.7 127.6 %while.15 = (s32[]{:T(128)}, f32[4,384]{1,0:T(4,128)S(1)}, f32[4,384]{1,0:T(4,128)S(1)}, f32[4,384,64]{1,2,0:T(8,128)S(1)}, bf16[12,1024,128]{2,1,0:T(8,128)(2,1...) while((s32[]{:T(128)}, f32[4,384]{1,0:T(4,128)S(1)}, f32[4,384]{1,0:T(4,128)S(1)}, ...), condition=%wide.region_5.6_spmd.clone, body=%wide.region_2.5_spmd.clone.sunk | while | flops 415538688 | bytes 46432384 | solution.py:134
  319.9 3.6 bitcast_reduce_fusion.3
  323.6 4.0 fusion.108
  330.6 3.6 bitcast_reduce_fusion.3
  334.2 4.0 fusion.108
  338.8 1.3 fusion.110
  341.2 3.6 bitcast_reduce_fusion.3
  344.8 4.0 fusion.108
  349.4 1.3 fusion.110
  351.8 3.6 bitcast_reduce_fusion.3
  355.4 4.0 fusion.108
  360.0 1.3 fusion.110
  362.4 3.6 bitcast_reduce_fusion.3
  366.1 4.0 fusion.108
  373.1 3.6 bitcast_reduce_fusion.3
  376.7 4.0 fusion.108
  381.3 1.3 fusion.110
  383.7 3.6 bitcast_reduce_fusion.3
  387.3 4.0 fusion.108
  391.9 1.3 fusion.110
  394.3 3.6 bitcast_reduce_fusion.3
  397.9 4.0 fusion.108
  404.9 3.6 bitcast_reduce_fusion.3
  408.6 4.0 fusion.108
  415.6 3.6 bitcast_reduce_fusion.3
  419.2 4.0 fusion.108
  423.8 1.3 fusion.110
  426.2 3.6 bitcast_reduce_fusion.3
  429.8 4.0 fusion.108
  434.4 1.3 fusion.110
  436.8 3.6 bitcast_reduce_fusion.3
  440.4 4.0 fusion.108
  446.4 1.8 convolution_convert_fusion.1
  448.2 4.1 all-to-all-start
  452.3 5.7 reduce_sum.96
  458.0 3.6 all_to_all.28
  461.6 10.4 %all-to-all-done = bf16[4,96,2048]{2,1,0:T(8,128)(2,1)S(1)} async-done(((bf16[4,96,2048]{2,1,0:T(8,128)(2,1)}), bf16[4,96,2048]{2,1,0:T(8,128)(2,1)S(1)}, u32[]{:S(2)}, u32[]{:S(2)}) %all-to-all-start) | async-done | bytes 1572896 | tf_op jit(solution)/shard_map/all_to_all | solution.py:52
  472.0 8.5 %all-to-all-start.5 = ((bf16[32,12,2048]{2,1,0:T(8,128)(2,1)}), bf16[32,12,2048]{2,1,0:T(8,128)(2,1)}, u32[]{:S(2)}, u32[]{:S(2)}) async-start(bf16[32,12,2048]{2,1,0:T(8,128)(2,1)} %all_to_all.28), calls=%async_computation.5 | async-start | bytes 4194304 | tf_op jit(solution)/shard_map/all_to_all | solution.py:237
  480.8 2.1 convert_reduce_fusion
  484.0 95.3 %all-to-all-done.5 = bf16[32,12,2048]{2,1,0:T(8,128)(2,1)} async-done(((bf16[32,12,2048]{2,1,0:T(8,128)(2,1)}), bf16[32,12,2048]{2,1,0:T(8,128)(2,1)}, u32[]{:S(2)}, u32[]{:S(2)}) %all-to-all-start.5) | async-done | bytes 1572896 | tf_op jit(solution)/shard_map/all_to_all | solution.py:237
  579.3 2.5 all_to_all.30
  581.8 1.7 gather_fusion.1
  583.5 4.0 gather_fusion.2
  587.5 2.4 add_convert_fusion
  (205 shorter events, 56.9 us)
Async XLA Ops:
  7.2 276.8 %copy-start = (bf16[2,256,2048]{2,1,0:T(8,128)(2,1)S(1)}, bf16[2,256,2048]{2,1,0:T(8,128)(2,1)}, u32[]{:S(2)}) copy-start(bf16[2,256,2048]{2,1,0:T(8,128)(2,1)} %param.30) | copy-start | bytes 6291460
  7.2 3.6 copy-start.8
  7.2 5.3 copy-start.4
  7.2 5.5 copy-start.7
  7.2 101.6 %all-gather.8.cloned.1.call-start = ((), (), s32[]{:S(2)}) async-start(), calls=%async_computation.7 | async-start | bytes 1671168 | tf_op jit(solution)/shard_map/all_gather | solution.py:24
  38.0 129.4 %all-to-all-start.3 = ((bf16[32,1,12,2048]{3,2,1,0:T(8,128)(2,1)}), bf16[32,1,12,2048]{3,2,1,0:T(8,128)(2,1)}, u32[]{:S(2)}, u32[]{:S(2)}) async-start(bf16[32,1,12,2048]{3,2,1,0:T(8,128)(2,1)} %fusion.41), calls=%async_computation.3 | async-start | bytes 4194304 | tf_op jit(solution)/shard_map/all_to_all | solution.py:221
  63.5 166.2 %all-gather.10.cloned.1.call-start = ((), (), s32[]{:S(2)}) async-start(), calls=%async_computation.8 | async-start | bytes 4718592 | tf_op jit(solution)/shard_map/all_gather | solution.py:24
  111.5 166.0 %all-gather.6.cloned.1.call-start = ((), (), s32[]{:S(2)}) async-start(), calls=%async_computation.6 | async-start | bytes 7864320 | tf_op jit(solution)/shard_map/all_gather | solution.py:225
  172.8 4.7 copy-start.6
  172.8 5.1 copy-start.10
  172.8 44.2 %all-to-all-start.1 = ((bf16[4,128,2048]{2,1,0:T(8,128)(2,1)}), bf16[4,128,2048]{2,1,0:T(8,128)(2,1)}, u32[]{:S(2)}, u32[]{:S(2)}) async-start(bf16[4,128,2048]{2,1,0:T(8,128)(2,1)} %broadcast_in_dim.47), calls=%async_computation.1 | async-start | bytes 4194304 | tf_op jit(solution)/shard_map/all_to_all | solution.py:37
  224.9 88.5 %all-to-all-start.2 = ((bf16[4,128,2048]{2,1,0:T(8,128)(2,1)}), bf16[4,128,2048]{2,1,0:T(8,128)(2,1)}, u32[]{:S(2)}, u32[]{:S(2)}) async-start(bf16[4,128,2048]{2,1,0:T(8,128)(2,1)} %bitcast.276), calls=%async_computation.2 | async-start | bytes 4194304 | tf_op jit(solution)/shard_map/all_to_all | solution.py:52
  313.4 134.8 %all-to-all-start.4 = ((bf16[4,384,2048]{2,1,0:T(8,128)(2,1)}), bf16[4,384,2048]{2,1,0:T(8,128)(2,1)}, u32[]{:S(2)}, u32[]{:S(2)}) async-start(bf16[4,384,2048]{2,1,0:T(8,128)(2,1)} %copy.99), calls=%async_computation.4 | async-start | bytes 12582912 | tf_op jit(solution)/shard_map/all_to_all | solution.py:52
  318.7 127.7 %copy-start.5 = (bf16[256,2048]{1,0:T(8,128)(2,1)S(1)}, bf16[256,2048]{1,0:T(8,128)(2,1)}, u32[]{:S(2)}) copy-start(bf16[256,2048]{1,0:T(8,128)(2,1)} %param.23) | copy-start | bytes 3145732
  323.5 4.6 copy-start.2
  334.2 4.6 copy-start.2
  344.8 4.6 copy-start.2
  355.4 4.6 copy-start.2
  366.0 4.6 copy-start.2
  376.7 4.6 copy-start.2
  387.3 4.6 copy-start.2
  397.9 4.6 copy-start.2
  408.5 4.6 copy-start.2
  419.2 4.6 copy-start.2
  429.8 4.6 copy-start.2
  440.4 4.6 copy-start.2
  448.2 23.8 %all-to-all-start = ((bf16[4,96,2048]{2,1,0:T(8,128)(2,1)}), bf16[4,96,2048]{2,1,0:T(8,128)(2,1)S(1)}, u32[]{:S(2)}, u32[]{:S(2)}) async-start(bf16[4,96,2048]{2,1,0:T(8,128)(2,1)} %bitcast.280), calls=%async_computation | async-start | bytes 3145728 | tf_op jit(solution)/shard_map/all_to_all | solution.py:52
  461.6 19.2 %copy-start.9 = (f32[128,2]{0,1:T(2,128)S(1)}, f32[128,2]{0,1:T(2,128)}, u32[]{:S(2)}) copy-start(f32[128,2]{0,1:T(2,128)} %param.27) | copy-start | bytes 3076
  472.0 107.2 %all-to-all-start.5 = ((bf16[32,12,2048]{2,1,0:T(8,128)(2,1)}), bf16[32,12,2048]{2,1,0:T(8,128)(2,1)}, u32[]{:S(2)}, u32[]{:S(2)}) async-start(bf16[32,12,2048]{2,1,0:T(8,128)(2,1)} %all_to_all.28), calls=%async_computation.5 | async-start | bytes 4194304 | tf_op jit(solution)/shard_map/all_to_all | solution.py:237
  581.8 1.7 copy-start.3
  583.5 6.4 %copy-start.1 = (bf16[2,256,2048]{2,1,0:T(8,128)(2,1)S(1)}, bf16[2,256,2048]{2,1,0:T(8,128)(2,1)}, u32[]{:S(2)}) copy-start(bf16[2,256,2048]{2,1,0:T(8,128)(2,1)} %param.30) | copy-start | bytes 6291460
Sparse Core Ops, SparseCore 0:
  10.9 97.9 all-gather.7
  111.6 33.0 all-gather.9
  171.2 106.2 all-gather.5
